TPU v7x, 32 devices: a whole 2x2x4 slice. The times are simulated.
32 devices in a mesh: sp: 8 (over z, y), tp: 4 (over x, core).
Axes of the slice: x: 2, y: 2, z: 4, core: 2. Of those that a mesh axis runs over, the one named last changes fastest.
Arguments:
- queries: bfloat16 [6144, 1536], P('sp', 'tp'), may hold values from -130 to 130, as said below
- keys: bfloat16 [6144, 512], P('sp', 'tp'), may hold values from -6 to 6
- values: bfloat16 [6144, 512], P('sp', 'tp'), may hold values from -6 to 6
- residual: bfloat16 [6144, 2048], P(('sp', 'tp')), may hold values from -6 to 6
- sinks: float32 [12], P('tp'), may hold values from 2 to 6
- out_weight: bfloat16 [1536, 2048], P('tp'), may hold values from -0.15625 to 0.15625
- up_weight: bfloat16 [2048, 8192], P('sp', 'tp'), may hold values from -0.125 to 0.125
- down_weight: bfloat16 [8192, 2048], P('tp', 'sp'), may hold values from -0.0625 to 0.0625
- gains: float32 [2, 2048], replicated, may hold values from 0.1 to 1.9
- biases: float32 [2, 2048], replicated, may hold values from -3 to 3
Outputs:
- layer_out: bfloat16 [6144, 2048], P(('sp', 'tp'))
Inputs may be any that keep to these rules, and one draw needn't show every extreme that they name: `queries`: entries of order one, with some rows far larger in some draws.
All inputs are finite; a program needn't handle non-finite values.
Results may differ from a plain program's by a relative error of at most 0.0095.
Values may be sent and summed in bfloat16 or wider, within the bound.
A program may use at most 128 MiB of HBM per device.

v0:
```python
import jax
import jax.numpy as jnp
from jax import lax
from jax.sharding import PartitionSpec as P

HEADS = 12
HEAD = 128
WINDOW = 128
deep_alpha = 1.6817928
norm_eps = 1e-05
neg_big = -1e30


def from_behind(block, axis, distance):
    devices = range(lax.axis_size(axis))
    route = [(i - distance, i) for i in devices if i - distance in devices]
    return lax.ppermute(block, axis, route)


def layer_norm(stream, gain, bias):
    mean = jnp.mean(stream, axis=-1, keepdims=True)
    spread = jnp.mean(jnp.square(stream - mean), axis=-1, keepdims=True)
    return ((stream - mean) * lax.rsqrt(spread + norm_eps) * gain + bias).astype(jnp.bfloat16)


def attend(queries, keys, values, before, sinks, offset, rank_tp):
    tokens = keys.shape[0]
    kv_local = keys.shape[1] // HEAD
    heads_local = sinks.shape[0]
    group = heads_local // kv_local
    blocks = tokens // WINDOW
    q_blocks = queries.reshape(blocks, WINDOW, kv_local, group, HEAD)
    key_ext = jnp.concatenate([before[0], keys], axis=0).reshape(tokens + WINDOW, kv_local, HEAD)
    val_ext = jnp.concatenate([before[1], values], axis=0).reshape(tokens + WINDOW, kv_local, HEAD)
    key_win = jnp.concatenate(
        [
            key_ext[:tokens].reshape(blocks, WINDOW, kv_local, HEAD),
            key_ext[WINDOW:].reshape(blocks, WINDOW, kv_local, HEAD),
        ],
        axis=1,
    )
    val_win = jnp.concatenate(
        [
            val_ext[:tokens].reshape(blocks, WINDOW, kv_local, HEAD),
            val_ext[WINDOW:].reshape(blocks, WINDOW, kv_local, HEAD),
        ],
        axis=1,
    )
    logits = jnp.einsum(
        "nqkgd,nskd->nkgqs", q_blocks, key_win, preferred_element_type=jnp.float32
    ) * HEAD ** (-0.5)
    q_index = jnp.arange(WINDOW, dtype=jnp.int32)[:, None]
    k_index = jnp.arange(2 * WINDOW, dtype=jnp.int32)[None, :]
    dist = q_index + WINDOW - k_index
    block_id = jnp.arange(blocks, dtype=jnp.int32)[:, None, None]
    key_pos = offset + block_id * WINDOW - WINDOW + k_index
    valid = (dist >= 0) & (dist < WINDOW) & (key_pos >= 0)
    heads = (jnp.arange(heads_local, dtype=jnp.int32) + rank_tp * heads_local).astype(jnp.float32)
    slopes = jnp.exp2(-8.0 * (heads + 1.0) / HEADS).reshape(kv_local, group)[:, :, None, None]
    logits = logits - slopes * dist.astype(jnp.float32)
    logits = jnp.where(valid[:, None, None], logits, neg_big)
    sink = sinks.reshape(kv_local, group)[:, :, None, None]
    top = jnp.maximum(jnp.max(logits, axis=-1, keepdims=True), sink)
    probs = jnp.exp(logits - top)
    denom = jnp.sum(probs, axis=-1, keepdims=True) + jnp.exp(sink - top)
    weight = (probs / denom).astype(jnp.bfloat16)
    attended = jnp.einsum("nkgqs,nskd->nqkgd", weight, val_win, preferred_element_type=jnp.float32)
    return attended.astype(jnp.bfloat16).reshape(tokens, heads_local * HEAD)


def on_device(
    queries, keys, values, residual, sinks, out_weight, up_weight, down_weight, gains, biases
):
    tokens = queries.shape[0]
    rank_tp = lax.axis_index("tp")
    up_full, down_full = (
        lax.all_gather(up_weight, "sp", axis=0, tiled=True),
        lax.all_gather(down_weight, "sp", axis=1, tiled=True),
    )
    tails = jnp.stack([keys[tokens - WINDOW :], values[tokens - WINDOW :]])
    before = from_behind(tails, "sp", 1)
    offset = lax.axis_index("sp") * tokens
    attended = attend(queries, keys, values, before, sinks, offset, rank_tp)
    mix = lax.psum_scatter(
        jnp.dot(attended, out_weight, preferred_element_type=jnp.float32).astype(jnp.bfloat16),
        "tp",
        scatter_dimension=0,
        tiled=True,
    ).astype(jnp.float32)
    normed = layer_norm(deep_alpha * residual.astype(jnp.float32) + mix, gains[0], biases[0])
    whole = lax.all_gather(normed, "tp", axis=0, tiled=True)
    upward = jnp.dot(whole, up_full, preferred_element_type=jnp.float32)
    act = jnp.square(jax.nn.relu(upward)).astype(jnp.bfloat16)
    terms = jnp.dot(act, down_full, preferred_element_type=jnp.float32)
    ffn = lax.psum_scatter(
        terms.astype(jnp.bfloat16), "tp", scatter_dimension=0, tiled=True
    ).astype(jnp.float32)
    return layer_norm(deep_alpha * normed.astype(jnp.float32) + ffn, gains[1], biases[1])


def solution(mesh):
    return jax.shard_map(
        on_device,
        mesh=mesh,
        in_specs=(
            P("sp", "tp"),
            P("sp", "tp"),
            P("sp", "tp"),
            P(("sp", "tp"), None),
            P("tp"),
            P("tp", None),
            P("sp", "tp"),
            P("tp", "sp"),
            P(),
            P(),
        ),
        out_specs=P(("sp", "tp"), None),
        check_vma=False,
    )
```

profile of v0, /device:TPU:0, one launch (start us, length us, event | category | flops | bytes accessed | tf_op | source)
XLA Modules:
  0.0 408.7 jit_solution(9440139312392734191)
XLA Ops:
  6.5 0.0 copy-start
  6.5 0.0 copy-start.6
  6.5 0.0 copy-start.7
  6.5 0.0 reduce-scatter.3.cloned.1.call-start
  6.5 0.9 slice_bitcast_fusion.2
  7.5 0.6 pad_maximum_fusion.2
  8.1 5.5 %collective-permute-start = (bf16[2,128,128]{2,1,0:T(8,128)(2,1)}, bf16[2,128,128]{2,1,0:T(8,128)(2,1)}, u32[]{:S(2)}, u32[]{:S(2)}) collective-permute-start(bf16[2,128,128]{2,1,0:T(8,128)(2,1)} %pad_maximum_fusion.2), channel_id=1, source_target_pairs={{0,4},{4,8},{8,12},{12,16},{16,20},{20,24},{24,28},{1,5},{5,9},{9,... | collective-permute-start | bytes 196616 | tf_op jit(solution)/shard_map/ppermute | solution.py:17
  13.8 0.1 add_compare_fusion
  13.8 0.1 broadcast_multiply_fusion
  13.9 1.0 broadcast_and_fusion
  14.9 0.0 copy-done.7
  14.9 0.2 reshape.206
  15.1 0.0 copy-done.6
  15.1 0.2 copy.14
  15.3 0.0 collective-permute-done
  15.3 0.8 slice_bitcast_fusion.1
  16.1 0.9 pad_maximum_fusion
  17.0 0.0 copy-start.10
  17.0 1.7 fusion.21
  18.7 0.0 copy-start.5
  18.7 0.0 copy-done.10
  18.7 0.1 broadcast_maximum_fusion
  18.8 1.3 copy-done.5
  20.1 0.4 fusion.1
  20.4 0.1 exponential_add_fusion
  20.5 0.2 copy.13
  20.7 2.2 fusion.2
  22.9 0.4 copy.18
  23.3 0.0 copy-done
  23.3 3.5 convolution_convert_fusion.1
  26.8 0.0 copy-start.8
  26.8 0.0 copy-start.9
  26.8 0.0 copy-start.2
  26.8 0.0 reduce-scatter.3.cloned.1.call-update
  26.9 0.0 all-gather.4.cloned.1.call-start
  26.9 0.6 copy-done.8
  27.6 0.0 copy-done.9
  27.6 39.3 %reduce-scatter.3.cloned.1.call-done = bf16[192,2048]{1,0:T(8,128)(2,1)} async-done(((bf16[768,2048]{1,0:T(8,128)(2,1)}), bf16[192,2048]{1,0:T(8,128)(2,1)}) %reduce-scatter.3.cloned.1.call-update) | async-done | bytes 786448 | tf_op jit(solution)/shard_map/reduce_scatter | solution.py:84
  66.9 0.0 copy-done.2
  66.9 0.0 copy-start.3
  66.9 1.5 fusion.3
  68.5 0.0 copy-done.3
  68.5 0.4 multiply_reduce_fusion.1
  69.0 1.4 add_convert_fusion.1
  70.3 0.0 all-gather.4.cloned.1.call-update
  70.3 0.0 all-gather.6.cloned.1.call-start
  70.4 0.7 all-gather.6.cloned.1.call-update
  71.1 0.0 all-gather.8.cloned.1.call-start
  71.1 0.5 all-gather.8.cloned.1.call-update
  71.7 0.2 reduce-scatter.5.cloned.1.call-start
  71.9 27.1 %all-gather.4.cloned.1.call-done = bf16[768,2048]{1,0:T(8,128)(2,1)} async-done(((bf16[192,2048]{1,0:T(8,128)(2,1)}), bf16[768,2048]{1,0:T(8,128)(2,1)}) %all-gather.4.cloned.1.call-update) | async-done | bytes 3145744 | tf_op jit(solution)/shard_map/all_gather | solution.py:91
  99.0 126.6 %all-gather.6.cloned.1.call-done = bf16[2048,2048]{1,0:T(8,128)(2,1)} async-done(((bf16[256,2048]{1,0:T(8,128)(2,1)}), bf16[2048,2048]{1,0:T(8,128)(2,1)}) %all-gather.6.cloned.1.call-update) | async-done | bytes 8388624 | tf_op jit(solution)/shard_map/all_gather | solution.py:77
  225.6 11.9 %multiply_convert_fusion = bf16[768,2048]{1,0:T(8,128)(2,1)} fusion(bf16[768,2048]{1,0:T(8,128)(2,1)} %all-gather.4.cloned.1.call-done, bf16[2048,2048]{1,0:T(8,128)(2,1)} %all-gather.6.cloned.1.call-done), kind=kOutput, calls=%fused_computation | convolution fusion | flops 6447169536 | bytes 14680064 | tf_op jit(solution)/shard_map/dot_general | solution.py:92
  237.5 113.2 %all-gather.8.cloned.1.call-done = bf16[2048,2048]{1,0:T(8,128)(2,1)} async-done(((bf16[2048,256]{1,0:T(8,128)(2,1)}), bf16[2048,2048]{1,0:T(8,128)(2,1)}) %all-gather.8.cloned.1.call-update) | async-done | bytes 8388624 | tf_op jit(solution)/shard_map/all_gather | solution.py:78
  350.7 11.8 %convolution_convert_fusion = bf16[768,2048]{1,0:T(8,128)(2,1)} fusion(bf16[768,2048]{1,0:T(8,128)(2,1)} %multiply_convert_fusion, bf16[2048,2048]{1,0:T(8,128)(2,1)} %all-gather.8.cloned.1.call-done), kind=kOutput, calls=%fused_computation.1 | convolution fusion | flops 6444023808 | bytes 14680064 | tf_op jit(solution)/shard_map/dot_general | solution.py:94
  362.5 0.0 copy-start.1
  362.5 0.0 reduce-scatter.5.cloned.1.call-update
  362.6 36.2 %reduce-scatter.5.cloned.1.call-done = bf16[192,2048]{1,0:T(8,128)(2,1)} async-done(((bf16[768,2048]{1,0:T(8,128)(2,1)}), bf16[192,2048]{1,0:T(8,128)(2,1)}) %reduce-scatter.5.cloned.1.call-update) | async-done | bytes 786448 | tf_op jit(solution)/shard_map/reduce_scatter | solution.py:95
  398.8 0.0 copy-done.1
  398.8 0.0 copy-start.4
  398.8 1.5 fusion.4
  400.3 0.0 copy-done.4
  400.3 0.4 multiply_reduce_fusion
  400.8 1.4 add_convert_fusion
  (12 shorter events, 0.2 us)
Async XLA Ops:
  6.5 16.8 %copy-start = (bf16[384,2048]{1,0:T(8,128)(2,1)S(1)}, bf16[384,2048]{1,0:T(8,128)(2,1)}, u32[]{:S(2)}) copy-start(bf16[384,2048]{1,0:T(8,128)(2,1)} %param.15) | copy-start | bytes 4718596
  6.5 8.5 %copy-start.6 = (bf16[768,128]{1,0:T(8,128)(2,1)S(1)}, bf16[768,128]{1,0:T(8,128)(2,1)}, u32[]{:S(2)}) copy-start(bf16[768,128]{1,0:T(8,128)(2,1)} %param.12) | copy-start | bytes 589828
  6.5 8.3 %copy-start.7 = (bf16[768,384]{1,0:T(8,128)(2,1)S(1)}, bf16[768,384]{1,0:T(8,128)(2,1)}, u32[]{:S(2)}) copy-start(bf16[768,384]{1,0:T(8,128)(2,1)} %param.10) | copy-start | bytes 1769476
  6.5 60.4 %reduce-scatter.3.cloned.1.call-start = ((), (), s32[]{:S(2)}) async-start(), calls=%async_computation.2 | async-start | bytes 3932160 | tf_op jit(solution)/shard_map/reduce_scatter | solution.py:84
  8.1 7.1 %collective-permute-start = (bf16[2,128,128]{2,1,0:T(8,128)(2,1)}, bf16[2,128,128]{2,1,0:T(8,128)(2,1)}, u32[]{:S(2)}, u32[]{:S(2)}) collective-permute-start(bf16[2,128,128]{2,1,0:T(8,128)(2,1)} %pad_maximum_fusion.2), channel_id=1, source_target_pairs={{0,4},{4,8},{8,12},{12,16},{16,20},{20,24},{24,28},{1,5},{5,9},{9,... | collective-permute-start | bytes 196616 | tf_op jit(solution)/shard_map/ppermute | solution.py:17
  17.0 1.7 copy-start.10
  18.7 1.4 copy-start.5
  26.8 0.7 copy-start.8
  26.8 0.7 copy-start.9
  26.8 40.1 %copy-start.2 = (bf16[192,2048]{1,0:T(8,128)(2,1)S(1)}, bf16[192,2048]{1,0:T(8,128)(2,1)}, u32[]{:S(2)}) copy-start(bf16[192,2048]{1,0:T(8,128)(2,1)} %param.13) | copy-start | bytes 2359300
  26.9 72.1 %all-gather.4.cloned.1.call-start = ((), (), s32[]{:S(2)}) async-start(), calls=%async_computation.3 | async-start | bytes 3932160 | tf_op jit(solution)/shard_map/all_gather | solution.py:91
  66.9 1.6 copy-start.3
  70.3 155.3 %all-gather.6.cloned.1.call-start = ((), (), s32[]{:S(2)}) async-start(), calls=%async_computation.4 | async-start | bytes 9437184 | tf_op jit(solution)/shard_map/all_gather | solution.py:77
  71.1 279.6 %all-gather.8.cloned.1.call-start = ((), (), s32[]{:S(2)}) async-start(), calls=%async_computation.5 | async-start | bytes 9437184 | tf_op jit(solution)/shard_map/all_gather | solution.py:78
  71.7 327.1 %reduce-scatter.5.cloned.1.call-start = ((), (), s32[]{:S(2)}) async-start(), calls=%async_computation.6 | async-start | bytes 3932160 | tf_op jit(solution)/shard_map/reduce_scatter | solution.py:95
  362.5 36.2 %copy-start.1 = (bf16[192,2048]{1,0:T(8,128)(2,1)S(1)}, bf16[192,2048]{1,0:T(8,128)(2,1)}, u32[]{:S(2)}) copy-start(bf16[192,2048]{1,0:T(8,128)(2,1)} %add_convert_fusion.1) | copy-start | bytes 2359300
  398.8 1.6 copy-start.4
Sparse Core Ops, SparseCore 0:
  27.0 39.9 reduce-scatter.2
  70.5 28.4 all-gather.3
  101.1 124.4 all-gather.5
  227.5 123.1 all-gather.7
  362.7 36.0 reduce-scatter.4
where the time goes:
time: 409 us
  waiting for transfers between devices  344 us (84%)
  matrix products  31.1 us (8%)
  between operations  13.3 us (3%)
  other arithmetic  10 us (2%)
  starting transfers between devices  5.86 us (1%)
  local copies, waits for them, and re-layouts  4.69 us (1%)
    all_gather x1, waiting for transfers between devices, on_device(): lax.all_gather(up_weight, 'sp', axis=0, tiled=True)  127 us
    all_gather x1, waiting for transfers between devices, on_device(): lax.all_gather(down_weight, 'sp', axis=1, tiled=True)  113 us
    reduce_scatter x1, waiting for transfers between devices, on_device(): lax.psum_scatter(jnp.dot(attended, out_weight, preferred_element_type=jnp...  39.3 us
    reduce_scatter x1, waiting for transfers between devices, on_device(): lax.psum_scatter(terms.astype(jnp.bfloat16), 'tp', scatter_dimension=0, t...  36.2 us
    all_gather x1, waiting for transfers between devices, on_device(): whole = lax.all_gather(normed, 'tp', axis=0, tiled=True)  27.1 us
    dot_general x1, matrix products, on_device(): upward = jnp.dot(whole, up_full, preferred_element_type=jnp.float32)  11.9 us
    dot_general x1, matrix products, on_device(): terms = jnp.dot(act, down_full, preferred_element_type=jnp.float32)  11.8 us
  transfers between devices with their start and end apart: 6, of which 5 were waited for; matrix products, arithmetic and copies ran while one was open for 3% of the time, Pallas kernels for 0%

commit v1 on v0

--- a/solution.py
+++ b/solution.py
@@ -2,6 +2,7 @@
 import jax.numpy as jnp
 from jax import lax
 from jax.sharding import PartitionSpec as P
+from jax.lax import all_gather
 
 HEADS = 12
 HEAD = 128
@@ -73,9 +74,13 @@
 ):
     tokens = queries.shape[0]
     rank_tp = lax.axis_index("tp")
+
+    def _turn_yards(inputs):
+        return jnp.concatenate(all_gather(inputs, "sp"), axis=1)
+
     up_full, down_full = (
         lax.all_gather(up_weight, "sp", axis=0, tiled=True),
-        lax.all_gather(down_weight, "sp", axis=1, tiled=True),
+        _turn_yards(down_weight),
     )
     tails = jnp.stack([keys[tokens - WINDOW :], values[tokens - WINDOW :]])
     before = from_behind(tails, "sp", 1)

time: 409 us -> 377 us (0.922)
  waiting for transfers between devices: 344 us -> 304 us
  local copies, waits for them, and re-layouts: 4.69 us -> 15.9 us
  matrix products: 31.1 us -> 25.7 us
    all_gather x1, waiting for transfers between devices: 113 us -> 84.6 us  [_turn_yards(): return jnp.concatenate(all_gather(inputs, 'sp'), axis=1)]
    reshape x0 -> x1, local copies, waits for them, and re-layouts: none -> 11.8 us  [_turn_yards(): return jnp.concatenate(all_gather(inputs, 'sp'), axis=1)]
    all_gather x1, waiting for transfers between devices: 27.1 us -> 16.2 us  [on_device(): whole = lax.all_gather(normed, 'tp', axis=0, tiled=True)]
  transfers between devices with their start and end apart: 6 -> 6, of which waited for: 5 -> 5; matrix products, arithmetic and copies ran while one was open for 3% -> 4% of each run, Pallas kernels for 0% -> 0%
where the time goes in v1:
time: 377 us; the launch traced here: 376 us
  waiting for transfers between devices  304 us (81%)
  matrix products  25.7 us (7%)
  local copies, waits for them, and re-layouts  15.9 us (4%)
  between operations  15.2 us (4%)
  other arithmetic  9.99 us (3%)
  starting transfers between devices  5.87 us (2%)
    all_gather x1, waiting for transfers between devices, on_device(): lax.all_gather(up_weight, 'sp', axis=0, tiled=True)  126 us
    all_gather x1, waiting for transfers between devices, _turn_yards(): return jnp.concatenate(all_gather(inputs, 'sp'), axis=1)  84.6 us
    reduce_scatter x1, waiting for transfers between devices, on_device(): lax.psum_scatter(jnp.dot(attended, out_weight, preferred_element_type=jnp...  39.3 us
    reduce_scatter x1, waiting for transfers between devices, on_device(): lax.psum_scatter(terms.astype(jnp.bfloat16), 'tp', scatter_dimension=0, t...  36.2 us
    all_gather x1, waiting for transfers between devices, on_device(): whole = lax.all_gather(normed, 'tp', axis=0, tiled=True)  16.2 us
    reshape x1, local copies, waits for them, and re-layouts, _turn_yards(): return jnp.concatenate(all_gather(inputs, 'sp'), axis=1)  11.8 us
    dot_general x1, matrix products, on_device(): upward = jnp.dot(whole, up_full, preferred_element_type=jnp.float32)  10.2 us
    dot_general x1, matrix products, on_device(): terms = jnp.dot(act, down_full, preferred_element_type=jnp.float32)  8.14 us
  transfers between devices with their start and end apart: 6, of which 5 were waited for; matrix products, arithmetic and copies ran while one was open for 4% of the time, Pallas kernels for 0%

profile of v1, /device:TPU:0, one launch (start us, length us, event | category | flops | bytes accessed | tf_op | source)
XLA Modules:
  0.0 376.3 jit_solution(1970613990248192173)
XLA Ops:
  7.4 0.0 copy-start
  7.4 0.0 copy-start.7
  7.4 0.0 copy-start.8
  7.4 0.0 reduce-scatter.3.cloned.1.call-start
  7.4 0.9 slice_bitcast_fusion.2
  8.3 0.6 pad_maximum_fusion.2
  8.9 5.5 %collective-permute-start = (bf16[2,128,128]{2,1,0:T(8,128)(2,1)}, bf16[2,128,128]{2,1,0:T(8,128)(2,1)}, u32[]{:S(2)}, u32[]{:S(2)}) collective-permute-start(bf16[2,128,128]{2,1,0:T(8,128)(2,1)} %pad_maximum_fusion.2), channel_id=1, source_target_pairs={{0,4},{4,8},{8,12},{12,16},{16,20},{20,24},{24,28},{1,5},{5,9},{9,... | collective-permute-start | bytes 196616 | tf_op jit(solution)/shard_map/ppermute | solution.py:18
  14.6 0.1 add_compare_fusion
  14.6 0.1 broadcast_multiply_fusion
  14.7 1.0 broadcast_and_fusion
  15.7 0.0 copy-done.8
  15.7 0.2 reshape.215
  15.9 0.0 copy-done.7
  15.9 0.2 copy.20
  16.1 0.0 collective-permute-done
  16.1 0.8 slice_bitcast_fusion.1
  16.9 0.9 pad_maximum_fusion
  17.8 0.0 copy-start.11
  17.8 1.7 fusion.21
  19.5 0.0 copy-start.6
  19.5 0.0 copy-done.11
  19.5 0.1 broadcast_maximum_fusion
  19.6 1.3 copy-done.6
  20.9 0.4 fusion.1
  21.2 0.1 exponential_add_fusion
  21.4 0.2 copy.19
  21.5 2.2 fusion.2
  23.7 0.4 copy.24
  24.1 0.0 copy-done
  24.2 3.6 convolution_convert_fusion.1
  27.7 0.0 copy-start.9
  27.7 0.0 copy-start.10
  27.7 0.0 reduce-scatter.3.cloned.1.call-update
  27.8 0.0 all-gather.9.cloned.1.call-start
  27.8 0.5 all-gather.9.cloned.1.call-update
  28.3 0.0 all-gather.5.cloned.1.call-start
  28.4 0.1 copy-done.9
  28.5 0.0 copy-done.10
  28.5 39.3 %reduce-scatter.3.cloned.1.call-done = bf16[192,2048]{1,0:T(8,128)(2,1)} async-done(((bf16[768,2048]{1,0:T(8,128)(2,1)}), bf16[192,2048]{1,0:T(8,128)(2,1)}) %reduce-scatter.3.cloned.1.call-update) | async-done | bytes 786448 | tf_op jit(solution)/shard_map/reduce_scatter | solution.py:89
  67.8 0.0 copy-done.3
  67.8 0.0 copy-start.4
  67.8 1.5 fusion.3
  69.4 0.0 copy-done.4
  69.4 0.4 multiply_reduce_fusion.1
  69.9 1.4 add_convert_fusion.1
  71.2 0.0 all-gather.5.cloned.1.call-update
  71.2 0.0 all-gather.7.cloned.1.call-start
  71.3 0.5 all-gather.7.cloned.1.call-update
  71.8 0.2 reduce-scatter.5.cloned.1.call-start
  72.0 84.6 %all-gather.9.cloned.1.call-done = bf16[16384,256]{1,0:T(8,128)(2,1)} async-done(((bf16[2048,256]{1,0:T(8,128)(2,1)}), bf16[16384,256]{1,0:T(8,128)(2,1)}) %all-gather.9.cloned.1.call-update) | async-done | bytes 8388624 | tf_op jit(solution)/shard_map/all_gather | solution.py:79
  156.6 11.8 %copy.25 = bf16[2048,8,256]{0,2,1:T(8,128)(2,1)} copy(bf16[2048,8,256]{2,0,1:T(8,128)(2,1)} %bitcast.59) | data formatting | bytes 16777216 | tf_op jit(solution)/shard_map/reshape | solution.py:79
  168.4 16.2 %all-gather.5.cloned.1.call-done = bf16[768,2048]{1,0:T(8,128)(2,1)} async-done(((bf16[192,2048]{1,0:T(8,128)(2,1)}), bf16[768,2048]{1,0:T(8,128)(2,1)}) %all-gather.5.cloned.1.call-update) | async-done | bytes 3145744 | tf_op jit(solution)/shard_map/all_gather | solution.py:96
  184.6 126.2 %all-gather.7.cloned.1.call-done = bf16[2048,2048]{1,0:T(8,128)(2,1)} async-done(((bf16[256,2048]{1,0:T(8,128)(2,1)}), bf16[2048,2048]{1,0:T(8,128)(2,1)}) %all-gather.7.cloned.1.call-update) | async-done | bytes 8388624 | tf_op jit(solution)/shard_map/all_gather | solution.py:82
  310.8 0.0 copy-start.2
  310.8 10.2 %multiply_convert_fusion = bf16[768,2048]{1,0:T(8,128)(2,1)S(1)} fusion(bf16[768,2048]{1,0:T(8,128)(2,1)} %all-gather.5.cloned.1.call-done, bf16[2048,2048]{1,0:T(8,128)(2,1)} %all-gather.7.cloned.1.call-done), kind=kOutput, calls=%fused_computation | convolution fusion | flops 6447169536 | bytes 14680064 | tf_op jit(solution)/shard_map/dot_general | solution.py:97
  321.0 0.0 copy-done.2
  321.0 8.1 %convolution_convert_fusion = bf16[768,2048]{1,0:T(8,128)(2,1)} fusion(bf16[768,2048]{1,0:T(8,128)(2,1)S(1)} %multiply_convert_fusion, bf16[2048,2048]{0,1:T(8,128)(2,1)S(1)} %bitcast.60), kind=kOutput, calls=%fused_computation.1 | convolution fusion | flops 6444023808 | bytes 14680064 | tf_op jit(solution)/shard_map/dot_general | solution.py:99
  329.1 0.0 reduce-scatter.5.cloned.1.call-update
  329.1 36.2 %reduce-scatter.5.cloned.1.call-done = bf16[192,2048]{1,0:T(8,128)(2,1)} async-done(((bf16[768,2048]{1,0:T(8,128)(2,1)}), bf16[192,2048]{1,0:T(8,128)(2,1)}) %reduce-scatter.5.cloned.1.call-update) | async-done | bytes 786448 | tf_op jit(solution)/shard_map/reduce_scatter | solution.py:100
  365.3 0.0 copy-done.1
  365.3 1.5 fusion.4
  366.9 0.0 copy-done.5
  366.9 0.4 multiply_reduce_fusion
  367.4 1.4 add_convert_fusion
  (15 shorter events, 0.2 us)
Async XLA Ops:
  7.4 16.8 %copy-start = (bf16[384,2048]{1,0:T(8,128)(2,1)S(1)}, bf16[384,2048]{1,0:T(8,128)(2,1)}, u32[]{:S(2)}) copy-start(bf16[384,2048]{1,0:T(8,128)(2,1)} %param.15) | copy-start | bytes 4718596
  7.4 8.5 %copy-start.7 = (bf16[768,128]{1,0:T(8,128)(2,1)S(1)}, bf16[768,128]{1,0:T(8,128)(2,1)}, u32[]{:S(2)}) copy-start(bf16[768,128]{1,0:T(8,128)(2,1)} %param.12) | copy-start | bytes 589828
  7.4 8.3 %copy-start.8 = (bf16[768,384]{1,0:T(8,128)(2,1)S(1)}, bf16[768,384]{1,0:T(8,128)(2,1)}, u32[]{:S(2)}) copy-start(bf16[768,384]{1,0:T(8,128)(2,1)} %param.10) | copy-start | bytes 1769476
  7.4 60.5 %reduce-scatter.3.cloned.1.call-start = ((), (), s32[]{:S(2)}) async-start(), calls=%async_computation.2 | async-start | bytes 3932160 | tf_op jit(solution)/shard_map/reduce_scatter | solution.py:89
  8.9 7.1 %collective-permute-start = (bf16[2,128,128]{2,1,0:T(8,128)(2,1)}, bf16[2,128,128]{2,1,0:T(8,128)(2,1)}, u32[]{:S(2)}, u32[]{:S(2)}) collective-permute-start(bf16[2,128,128]{2,1,0:T(8,128)(2,1)} %pad_maximum_fusion.2), channel_id=1, source_target_pairs={{0,4},{4,8},{8,12},{12,16},{16,20},{20,24},{24,28},{1,5},{5,9},{9,... | collective-permute-start | bytes 196616 | tf_op jit(solution)/shard_map/ppermute | solution.py:18
  17.8 1.7 copy-start.11
  19.5 1.4 copy-start.6
  27.7 0.7 copy-start.9
  27.7 0.7 copy-start.10
  27.7 40.1 %copy-start.3 = (bf16[192,2048]{1,0:T(8,128)(2,1)S(1)}, bf16[192,2048]{1,0:T(8,128)(2,1)}, u32[]{:S(2)}) copy-start(bf16[192,2048]{1,0:T(8,128)(2,1)} %param.13) | copy-start | bytes 2359300
  27.8 128.8 %all-gather.9.cloned.1.call-start = ((), (), s32[]{:S(2)}) async-start(), calls=%async_computation.6 | async-start | bytes 9437184 | tf_op jit(solution)/shard_map/all_gather | solution.py:79
  28.3 156.3 %all-gather.5.cloned.1.call-start = ((), (), s32[]{:S(2)}) async-start(), calls=%async_computation.3 | async-start | bytes 3932160 | tf_op jit(solution)/shard_map/all_gather | solution.py:96
  67.8 1.6 copy-start.4
  71.2 239.6 %all-gather.7.cloned.1.call-start = ((), (), s32[]{:S(2)}) async-start(), calls=%async_computation.4 | async-start | bytes 9437184 | tf_op jit(solution)/shard_map/all_gather | solution.py:82
  71.8 293.5 %reduce-scatter.5.cloned.1.call-start = ((), (), s32[]{:S(2)}) async-start(), calls=%async_computation.5 | async-start | bytes 3932160 | tf_op jit(solution)/shard_map/reduce_scatter | solution.py:100
  310.8 10.2 %copy-start.2 = (bf16[2048,8,256]{0,2,1:T(8,128)(2,1)S(1)}, bf16[2048,8,256]{0,2,1:T(8,128)(2,1)}, u32[]{:S(2)}) copy-start(bf16[2048,8,256]{0,2,1:T(8,128)(2,1)} %copy.25) | copy-start | bytes 25165828
  329.1 36.2 %copy-start.1 = (bf16[192,2048]{1,0:T(8,128)(2,1)S(1)}, bf16[192,2048]{1,0:T(8,128)(2,1)}, u32[]{:S(2)}) copy-start(bf16[192,2048]{1,0:T(8,128)(2,1)} %add_convert_fusion.1) | copy-start | bytes 2359300
  365.3 1.6 copy-start.5
Sparse Core Ops, SparseCore 0:
  27.9 39.9 reduce-scatter.2
  329.3 36.0 reduce-scatter.4
Sparse Core Ops, SparseCore 1:
  30.4 126.2 all-gather.8
  158.0 26.5 all-gather.4
  186.6 124.1 all-gather.6
